TPU v7x, 32 devices: a whole 2x2x4 slice. The times are simulated.
32 devices in a mesh: grp: 2 (over y), sp: 4 (over z), tp: 4 (over x, core).
Axes of the slice: x: 2, y: 2, z: 4, core: 2. Of those that a mesh axis runs over, the one named last changes fastest.
Arguments:
- tokens: bfloat16 [3072, 2048], P(('grp', 'sp'), 'tp'), parts along dimension 0, may hold values from -6 to 6
- norm_gain: float32 [2048], replicated, may hold values from 0.1 to 1.9
- qk_gain: float32 [4, 64], replicated, may hold values from 0.7 to 5.5
- w_query_window: bfloat16 [2048, 1024], P('sp', 'tp'), may hold values from -1 to 1
- w_key_window: bfloat16 [2048, 512], P('sp', 'tp'), may hold values from -1 to 1
- w_value_window: bfloat16 [2048, 512], P('sp', 'tp'), may hold values from -0.125 to 0.125
- sink_logits: float32 [16], P('tp'), may hold values from 0 to 5
- w_query_forget: bfloat16 [2048, 1024], P('sp', 'tp'), may hold values from -1 to 1
- w_key_forget: bfloat16 [2048, 1024], P('sp', 'tp'), may hold values from -1 to 1
- w_value_forget: bfloat16 [2048, 1024], P('sp', 'tp'), may hold values from -0.125 to 0.125
- gate_cum: float32 [3072, 16], P(('grp', 'sp'), 'tp'), parts along dimension 0, as said below
- w_merge: bfloat16 [2048, 2, 2048], P('sp', None, 'tp'), may hold values from -0.125 to 0.125
- w_branch: bfloat16 [2, 1024, 2048], P(None, 'sp', 'tp'), may hold values from -0.8984375 to 0.8984375
Outputs:
- mixed: bfloat16 [3072, 2048], P(('grp', 'sp'), 'tp'), parts along dimension 0
There are 2 independent parts, one for each index of `grp`. A program takes and returns all parts, laid end to end along the dimension named above; an argument that names none is the same for every part. Nothing has to cross between parts.
Inputs may be any that keep to these rules, and one draw needn't show every extreme that they name: `gate_cum`: along positions each head's values never rise.
All inputs are finite; a program needn't handle non-finite values.
Results may differ from a plain program's by a relative error of at most 0.012.
Values may be sent and summed in bfloat16 or wider, within the bound.
A program may use at most 64 MiB of HBM per device.

v0:
```python
import math
import jax
import jax.numpy as jnp
from jax import lax
from jax.sharding import PartitionSpec as P

HEAD = 64
WINDOW = 128
epsilon = 1e-06
big_negative = -1e30


def from_behind(value, axis, by):
    size = lax.axis_size(axis)
    pairs = [(i, i + by) for i in range(size) if 0 <= i + by < size]
    return lax.ppermute(value, axis, pairs)


def head_norm(raw, gain, head_count):
    split = raw.reshape(raw.shape[0], head_count, -1)
    scaled = split * lax.rsqrt(jnp.mean(split * split, axis=-1, keepdims=True) + epsilon) * gain
    return scaled.astype(jnp.bfloat16)


def window_attend(queries, keys_ext, values_ext, sink_rows, first_pos):
    row_count, head_count, head_size = queries.shape
    group_count = keys_ext.shape[1]
    span_rows = WINDOW // 2
    block_count = row_count // span_rows
    query_blocks = queries.reshape(
        block_count, span_rows, group_count, head_count // group_count, head_size
    )
    key_blocks = jnp.concatenate(
        [
            keys_ext[lag_index * span_rows : lag_index * span_rows + row_count].reshape(
                block_count, span_rows, group_count, head_size
            )
            for lag_index in range(3)
        ],
        axis=1,
    )
    value_blocks = jnp.concatenate(
        [
            values_ext[lag_index * span_rows : lag_index * span_rows + row_count].reshape(
                block_count, span_rows, group_count, head_size
            )
            for lag_index in range(3)
        ],
        axis=1,
    )
    scores = jnp.einsum(
        "nqgrd,nkgd->ngrqk", query_blocks, key_blocks, preferred_element_type=jnp.float32
    ) * head_size ** (-0.5)
    distance = WINDOW + jnp.arange(span_rows)[:, None] - jnp.arange(3 * span_rows)[None, :]
    key_pos = (
        first_pos
        - WINDOW
        + jnp.arange(block_count)[:, None] * span_rows
        + jnp.arange(3 * span_rows)[None, :]
    )
    is_valid = ((distance >= 0) & (distance < WINDOW))[None] & (key_pos >= 0)[:, None, :]
    is_valid = is_valid[:, None, None]
    sink_grid = sink_rows.reshape(1, group_count, head_count // group_count, 1)
    row_max = jnp.maximum(jnp.max(jnp.where(is_valid, scores, big_negative), axis=-1), sink_grid)
    weights = jnp.where(is_valid, jnp.exp(scores - row_max[..., None]), 0.0)
    row_total = jnp.sum(weights, axis=-1) + jnp.exp(sink_grid - row_max)
    prob_rows = (weights / row_total[..., None]).astype(jnp.bfloat16)
    mixed_sum = jnp.einsum(
        "ngrqk,nkgd->nqgrd", prob_rows, value_blocks, preferred_element_type=jnp.float32
    )
    return mixed_sum.reshape(row_count, head_count * head_size).astype(jnp.bfloat16)


def forget_groups(groups, keys, values, gates):
    head_count, head_size = (keys.shape[1], keys.shape[2])
    gates_all = lax.all_gather(gates, "sp", axis=0, tiled=True)

    def absorber(queries, query_gate, query_pos):

        def absorb(running, block):
            row_max, row_total, mixed_sum = running
            key_rows, value_rows, key_gate, key_pos = block
            scores = jnp.einsum(
                "qhd,khd->hqk", queries, key_rows, preferred_element_type=jnp.float32
            ) * head_size ** (-0.5)
            scores = scores + query_gate.T[:, :, None] - key_gate.T[:, None, :]
            is_valid = (query_pos[:, None] >= key_pos[None, :])[None]
            new_max = jnp.maximum(
                row_max, jnp.max(jnp.where(is_valid, scores, big_negative), axis=-1)
            )
            weights = jnp.where(is_valid, jnp.exp(scores - new_max[..., None]), 0.0)
            shrink = jnp.exp(row_max - new_max)
            row_total = row_total * shrink + jnp.sum(weights, axis=-1)
            mixed_sum = mixed_sum * shrink.T[:, :, None] + jnp.einsum(
                "hqk,khd->qhd",
                weights.astype(jnp.bfloat16),
                value_rows,
                preferred_element_type=jnp.float32,
            )
            return ((new_max, row_total, mixed_sum), None)

        return absorb

    initial = tuple(
        (
            (
                jnp.full((head_count, group[0].shape[0]), big_negative, jnp.float32),
                jnp.zeros((head_count, group[0].shape[0]), jnp.float32),
                jnp.zeros((group[0].shape[0], head_count, head_size), jnp.float32),
            )
            for group in groups
        )
    )
    first_row = jnp.int32(0)
    key_rows = lax.all_gather(keys, "sp", axis=0, tiled=True)
    value_rows = lax.all_gather(values, "sp", axis=0, tiled=True)
    piece_rows = key_rows.shape[0]
    sub_rows = math.gcd(piece_rows, 2048)
    turns = piece_rows // sub_rows
    key_gate = gates_all
    key_pos = jnp.arange(piece_rows)
    blocks = (
        key_rows.reshape(turns, sub_rows, head_count, head_size),
        value_rows.reshape(turns, sub_rows, head_count, head_size),
        key_gate.reshape(turns, sub_rows, head_count),
        key_pos.reshape(turns, sub_rows),
    )
    updated = []
    for (queries, query_gate, query_pos), state in zip(groups, initial):
        absorb = absorber(queries, query_gate, query_pos)

        def advance(current):
            return lax.scan(absorb, current, blocks)[0]

        def keep(current):
            return current

        updated.append(lax.cond(first_row <= query_pos[-1], advance, keep, state))
    finals = tuple(updated)
    return [
        (mixed_sum / row_total.T[:, :, None])
        .reshape(mixed_sum.shape[0], head_count * head_size)
        .astype(jnp.bfloat16)
        for row_max, row_total, mixed_sum in finals
    ]


def on_device(
    tokens,
    norm_gain,
    qk_gain,
    w_query_window,
    w_key_window,
    w_value_window,
    sink_logits,
    w_query_forget,
    w_key_forget,
    w_value_forget,
    gate_cum,
    w_merge,
    w_branch,
):
    row_count = tokens.shape[0]
    row_offset = lax.axis_index("sp") * row_count
    gathered = lax.all_gather(tokens, "tp", axis=1, tiled=True)
    as_float = gathered.astype(jnp.float32)
    normed = (
        as_float
        * lax.rsqrt(jnp.mean(as_float * as_float, axis=-1, keepdims=True) + epsilon)
        * norm_gain
    ).astype(jnp.bfloat16)
    merge_flat = w_merge.reshape(w_merge.shape[0], -1)
    pieces = (
        lax.all_gather(w_query_window, "sp", axis=0, tiled=True),
        lax.all_gather(w_key_window, "sp", axis=0, tiled=True),
        lax.all_gather(w_value_window, "sp", axis=0, tiled=True),
        lax.all_gather(w_query_forget, "sp", axis=0, tiled=True),
        lax.all_gather(w_key_forget, "sp", axis=0, tiled=True),
        lax.all_gather(w_value_forget, "sp", axis=0, tiled=True),
        lax.all_gather(merge_flat, "sp", axis=0, tiled=True),
    )
    projected = tuple(
        (jnp.dot(normed, weight_rows, preferred_element_type=jnp.float32) for weight_rows in pieces)
    )
    query_heads = w_query_window.shape[1] // HEAD
    group_heads = w_key_window.shape[1] // HEAD
    window_query = head_norm(projected[0], qk_gain[0], query_heads)
    window_key = head_norm(projected[1], qk_gain[1], group_heads)
    window_value = projected[2].astype(jnp.bfloat16).reshape(row_count, group_heads, HEAD)
    prev_key, prev_value = from_behind(
        (window_key[row_count - WINDOW :], window_value[row_count - WINDOW :]), "sp", 1
    )
    window_out = window_attend(
        window_query,
        jnp.concatenate([prev_key, window_key], axis=0),
        jnp.concatenate([prev_value, window_value], axis=0),
        sink_logits,
        row_offset,
    )
    forget_query = head_norm(projected[3], qk_gain[2], query_heads)
    forget_key = head_norm(projected[4], qk_gain[3], query_heads)
    forget_value = projected[5].astype(jnp.bfloat16).reshape(row_count, query_heads, HEAD)
    own_pos = row_offset + jnp.arange(row_count)
    forget_out = forget_groups(
        [(forget_query, gate_cum, own_pos)], forget_key, forget_value, gate_cum
    )[0]
    channel_count = w_merge.shape[2]
    merge_gate = jax.nn.sigmoid(projected[6]).reshape(row_count, 2, channel_count)
    branch_full = lax.all_gather(w_branch, "sp", axis=1, tiled=True)
    head_stack = jnp.stack([window_out, forget_out], axis=1)
    weight_rows = branch_full
    projection = jnp.einsum(
        "uxa,xag->uxg",
        lax.all_gather(head_stack, "tp", axis=2, tiled=True),
        weight_rows,
        preferred_element_type=jnp.float32,
    )
    return (merge_gate[:, 0] * projection[:, 0] + merge_gate[:, 1] * projection[:, 1]).astype(
        jnp.bfloat16
    )


def solution(mesh):
    return jax.shard_map(
        on_device,
        mesh=mesh,
        in_specs=(
            P(("grp", "sp"), "tp"),
            P(),
            P(),
            P("sp", "tp"),
            P("sp", "tp"),
            P("sp", "tp"),
            P("tp"),
            P("sp", "tp"),
            P("sp", "tp"),
            P("sp", "tp"),
            P(("grp", "sp"), "tp"),
            P("sp", None, "tp"),
            P(None, "sp", "tp"),
        ),
        out_specs=P(("grp", "sp"), "tp"),
        check_vma=False,
    )
```

profile of v0, /device:TPU:0, one launch (start us, length us, event | category | flops | bytes accessed | tf_op | source)
XLA Modules:
  0.0 339.6 jit_solution(14842164746860835694)
XLA Ops:
  6.6 0.7 all-gather.9.cloned.1.call-update
  7.3 0.7 all-gather.15.cloned.1.call-update
  8.1 0.7 all-gather.17.cloned.1.call-update
  11.2 1.3 slice.58
  13.7 16.6 %all_gather.48 = f32[1536,4]{0,1:T(4,128)} all-gather(f32[384,4]{0,1:T(4,128)} %param.27), channel_id=1, replica_groups=mesh['grp'=2,'sp'=4,'tp'=4] {'sp'}, dimensions={0}, use_global_device_ids=true | all-gather | bytes 30720 | tf_op jit(solution)/shard_map/all_gather | solution.py:76
  30.5 19.0 %all_gather.42 = bf16[2048,128]{1,0:T(8,128)(2,1)} all-gather(bf16[512,128]{1,0:T(8,128)(2,1)S(1)} %copy-done.8), channel_id=1, replica_groups=mesh['grp'=2,'sp'=4,'tp'=4] {'sp'}, dimensions={0}, use_global_device_ids=true | all-gather | bytes 655360 | tf_op jit(solution)/shard_map/all_gather | solution.py:175
  49.5 0.7 max.20
  50.2 21.1 %all_gather.41 = bf16[2048,128]{1,0:T(8,128)(2,1)} all-gather(bf16[512,128]{1,0:T(8,128)(2,1)S(1)} %copy-done.9), channel_id=1, replica_groups=mesh['grp'=2,'sp'=4,'tp'=4] {'sp'}, dimensions={0}, use_global_device_ids=true | all-gather | bytes 655360 | tf_op jit(solution)/shard_map/all_gather | solution.py:176
  71.2 0.7 broadcast_and_fusion
  71.9 1.9 fusion.25
  74.3 2.5 multiply_reduce_fusion.1
  77.0 25.4 %all_gather.45 = bf16[1536,4,64]{0,2,1:T(8,128)(2,1)S(1)} all-gather(bf16[384,4,64]{0,2,1:T(8,128)(2,1)S(1)} %multiply_convert_fusion.2), channel_id=1, replica_groups=mesh['grp'=2,'sp'=4,'tp'=4] {'sp'}, dimensions={0}, use_global_device_ids=true | all-gather | bytes 983040 | tf_op jit(solution)/shard_map/all_gather | solution.py:115
  102.5 5.3 %all-gather.17.cloned.1.call-done = bf16[2048,256]{1,0:T(8,128)(2,1)} async-done(((bf16[512,256]{1,0:T(8,128)(2,1)}), bf16[2048,256]{1,0:T(8,128)(2,1)}) %all-gather.17.cloned.1.call-update) | async-done | bytes 1048592 | tf_op jit(solution)/shard_map/all_gather | solution.py:179
  107.7 2.0 convolution_convert_fusion.1
  109.7 25.2 %all_gather.47 = bf16[1536,4,64]{0,2,1:T(8,128)(2,1)S(1)} all-gather(bf16[384,4,64]{0,2,1:T(8,128)(2,1)S(1)} %bitcast.165), channel_id=1, replica_groups=mesh['grp'=2,'sp'=4,'tp'=4] {'sp'}, dimensions={0}, use_global_device_ids=true | all-gather | bytes 983040 | tf_op jit(solution)/shard_map/all_gather | solution.py:116
  134.9 8.7 %all-gather.19.cloned.1.call-done = bf16[2048,256]{1,0:T(8,128)(2,1)} async-done(((bf16[512,256]{1,0:T(8,128)(2,1)}), bf16[2048,256]{1,0:T(8,128)(2,1)}) %all-gather.19.cloned.1.call-update) | async-done | bytes 1048592 | tf_op jit(solution)/shard_map/all_gather | solution.py:177
  143.7 2.1 multiply_reduce_fusion
  145.7 1.2 multiply_reduce_fusion.2
  147.0 1.2 convolution_convert_fusion.2
  148.2 0.8 multiply_convert_fusion.1
  149.0 35.5 %conditional.1 = (f32[4,384]{1,0:T(4,128)}, f32[384,4,64]{0,2,1:T(8,128)}) conditional(s32[]{:T(128)} %bitcast.13, () %tuple.20, (bf16[1536,4,64]{0,2,1:T(8,128)(2,1)S(1)}, bf16[1536,4,64]{0,2,1:T(8,128)(2,1)S(1)}, f32[1536,4]{0,1:T(4,128)}, s32[3,512]{1,0:T(4,128)S(1)}, s32[3,512]{1,0:T(4,128)S(1)}, /*index=5*/s32[384]{0:T(512)}, ...), branch_computations={%region_7.8_spmd, %region_8.13_spmd} | conditional | flops 215199744 | bytes 15060769 | solution.py:138
  149.6 1.4 copy_bitcast_fusion
  151.0 33.5 %while.18 = (s32[]{:T(128)}, f32[4,384]{1,0:T(4,128)S(1)}, f32[4,384]{1,0:T(4,128)}, f32[384,4,64]{0,2,1:T(8,128)}, s32[384]{0:T(512)}, /*index=5*/s32[3,512]{1,...) while((s32[]{:T(128)}, f32[4,384]{1,0:T(4,128)S(1)}, ...), condition=%wide.region_12.12_spmd.clone, body=%wide.region_9.11_spmd.clone.sunk | while | flops 215196672 | bytes 11896481 | solution.py:133
  151.0 0.7 dynamic-slice_bitcast_fusion.2
  151.7 0.7 constant_dynamic-slice_fusion.2
  152.4 0.9 broadcast_compare_fusion.2
  153.2 2.7 fusion.85
  155.9 0.7 fusion.86
  156.6 1.6 fusion.87
  158.2 0.6 fusion.88
  158.8 2.7 fusion.89
  161.6 0.7 dynamic-slice_bitcast_fusion.2
  162.3 0.7 constant_dynamic-slice_fusion.2
  163.0 0.9 broadcast_compare_fusion.2
  163.8 2.7 fusion.85
  166.5 0.7 fusion.86
  167.2 1.6 fusion.87
  168.8 1.3 fusion.88
  170.1 2.9 fusion.89
  173.0 0.7 dynamic-slice_bitcast_fusion.2
  173.7 0.7 constant_dynamic-slice_fusion.2
  174.4 0.9 broadcast_compare_fusion.2
  175.3 2.7 fusion.85
  178.0 0.7 fusion.86
  178.7 1.6 fusion.87
  180.3 1.3 fusion.88
  181.6 2.9 fusion.89
  184.5 1.0 divide_convert_fusion.2
  185.5 2.5 bitcast_reduce_fusion
  189.8 2.8 collective-permute-start.1
  192.6 3.3 collective-permute-start
  195.9 1.0 multiply_convert_fusion
  199.2 0.6 fusion.31
  200.0 1.0 fusion.32
  201.6 0.8 pad_maximum_fusion
  202.5 1.3 copy.55
  203.8 14.9 %all-gather.23.cloned.1.call-done = bf16[2,1024,512]{2,1,0:T(8,128)(2,1)} async-done(((bf16[2,256,512]{2,1,0:T(8,128)(2,1)}), bf16[2,1024,512]{2,1,0:T(8,128)(2,1)}) %all-gather.23.cloned.1.call-update) | async-done | bytes 2097168 | tf_op jit(solution)/shard_map/all_gather | solution.py:209
  218.6 21.5 %all-gather.21.cloned.1.call-done = bf16[384,2,1024]{2,0,1:T(8,128)(2,1)} async-done(((bf16[384,2,256]{2,0,1:T(8,128)(2,1)}), bf16[384,2,1024]{2,0,1:T(8,128)(2,1)}) %all-gather.21.cloned.1.call-update) | async-done | bytes 1572880 | tf_op jit(solution)/shard_map/all_gather | solution.py:214
  240.2 3.0 convolution_bitcast_fusion
  243.2 79.3 %all-gather.11.cloned.1.call-done = bf16[2048,1024]{1,0:T(8,128)(2,1)} async-done(((bf16[512,1024]{1,0:T(8,128)(2,1)}), bf16[2048,1024]{1,0:T(8,128)(2,1)}) %all-gather.11.cloned.1.call-update) | async-done | bytes 4194320 | tf_op jit(solution)/shard_map/all_gather | solution.py:180
  322.5 5.3 %add_divide_fusion = f32[384,1024]{1,0:T(8,128)} fusion(bf16[384,2048]{1,0:T(8,128)(2,1)S(1)} %copy-done.1, bf16[2048,1024]{1,0:T(8,128)(2,1)} %all-gather.11.cloned.1.call-done), kind=kOutput, calls=%fused_computation.44 | convolution fusion | flops 1611792384 | bytes 7340032 | tf_op jit(solution)/shard_map/dot_general | solution.py:183
  327.8 2.6 reshape.258
  330.5 1.2 fusion.56
  331.7 1.0 fusion.36
  (103 shorter events, 9.1 us)
Async XLA Ops:
  6.5 6.6 %copy-start.15 = (f32[4,64]{1,0:T(4,128)S(1)}, f32[4,64]{1,0:T(4,128)}, u32[]{:S(2)}) copy-start(f32[4,64]{1,0:T(4,128)} %param.19) | copy-start | bytes 3076
  6.5 24.0 %copy-start.8 = (bf16[512,128]{1,0:T(8,128)(2,1)S(1)}, bf16[512,128]{1,0:T(8,128)(2,1)}, u32[]{:S(2)}) copy-start(bf16[512,128]{1,0:T(8,128)(2,1)} %param.21) | copy-start | bytes 393220
  6.5 42.9 %copy-start.16 = (f32[4]{0:T(128)S(1)}, f32[4]{0:T(128)}, u32[]{:S(2)}) copy-start(f32[4]{0:T(128)} %param.23) | copy-start | bytes 52
  6.5 43.6 %copy-start.9 = (bf16[512,128]{1,0:T(8,128)(2,1)S(1)}, bf16[512,128]{1,0:T(8,128)(2,1)}, u32[]{:S(2)}) copy-start(bf16[512,128]{1,0:T(8,128)(2,1)} %param.22) | copy-start | bytes 393220
  6.5 65.4 %all-gather.9.cloned.1.call-start = ((), (), s32[]{:S(2)}) async-start(), calls=%async_computation | async-start | bytes 1966080 | tf_op jit(solution)/shard_map/all_gather | solution.py:165
  7.3 67.1 %all-gather.15.cloned.1.call-start = ((), (), s32[]{:S(2)}) async-start(), calls=%async_computation.3 | async-start | bytes 1310720 | tf_op jit(solution)/shard_map/all_gather | solution.py:178
  8.0 99.7 %all-gather.17.cloned.1.call-start = ((), (), s32[]{:S(2)}) async-start(), calls=%async_computation.4 | async-start | bytes 1310720 | tf_op jit(solution)/shard_map/all_gather | solution.py:179
  8.8 134.9 %all-gather.19.cloned.1.call-start = ((), (), s32[]{:S(2)}) async-start(), calls=%async_computation.5 | async-start | bytes 1310720 | tf_op jit(solution)/shard_map/all_gather | solution.py:177
  9.3 176.2 %all-gather.13.cloned.1.call-start = ((), (), s32[]{:S(2)}) async-start(), calls=%async_computation.2 | async-start | bytes 1310720 | tf_op jit(solution)/shard_map/all_gather | solution.py:174
  9.9 208.7 %all-gather.23.cloned.1.call-start = ((), (), s32[]{:S(2)}) async-start(), calls=%async_computation.7 | async-start | bytes 2621440 | tf_op jit(solution)/shard_map/all_gather | solution.py:209
  10.5 63.4 %copy-start.11 = (f32[2048]{0:T(1024)S(1)}, f32[2048]{0:T(1024)}, u32[]{:S(2)}) copy-start(f32[2048]{0:T(1024)} %param.18) | copy-start | bytes 24580
  10.5 229.6 %all-gather.21.cloned.1.call-start = ((), (), s32[]{:S(2)}) async-start(), calls=%async_computation.6 | async-start | bytes 1966080 | tf_op jit(solution)/shard_map/all_gather | solution.py:214
  71.9 1.9 copy-start.2
  74.3 72.6 %copy-start = (bf16[384,2048]{1,0:T(8,128)(2,1)}, bf16[384,2048]{1,0:T(8,128)(2,1)S(1)}, u32[]{:S(2)}) copy-start(bf16[384,2048]{1,0:T(8,128)(2,1)S(1)} %fusion.27) | copy-start | bytes 4718596
  143.7 2.1 copy-start.3
  145.7 1.2 copy-start.4
  185.5 2.6 copy-start.5
  188.4 1.1 copy-start.10
  188.4 1.2 copy-start.12
  188.6 7.3 %copy-start.14 = (f32[64]{0:T(128)S(1)}, f32[64]{0:T(128)}, u32[]{:S(2)}) copy-start(f32[64]{0:T(128)} %get-tuple-element.195) | copy-start | bytes 772
  189.8 7.2 %collective-permute-start.1 = (bf16[128,2,64]{0,2,1:T(8,128)(2,1)S(1)}, bf16[128,2,64]{0,2,1:T(8,128)(2,1)S(1)}, u32[]{:S(2)}, u32[]{:S(2)}) collective-permute-start(bf16[128,2,64]{0,2,1:T(8,128)(2,1)S(1)} %slice.68), channel_id=1, source_target_pairs={{0,4},{4,8},{8,12},{1,5},{5,9},{9,13},{2,6},{6,10},{10,14},{3,7},{... | collective-permute-start | bytes 98312 | tf_op jit(solution)/shard_map/ppermute | solution.py:16
  192.6 5.4 %collective-permute-start = (bf16[128,2,64]{0,2,1:T(8,128)(2,1)S(1)}, bf16[128,2,64]{0,2,1:T(8,128)(2,1)S(1)}, u32[]{:S(2)}, u32[]{:S(2)}) collective-permute-start(bf16[128,2,64]{0,2,1:T(8,128)(2,1)S(1)} %bitcast.167), channel_id=1, source_target_pairs={{0,4},{4,8},{8,12},{1,5},{5,9},{9,13},{2,6},{6,10},{10,14},{3,7},{... | collective-permute-start | bytes 98312 | tf_op jit(solution)/shard_map/ppermute | solution.py:16
  197.3 1.2 copy-start.7
  198.5 0.7 copy-start.13
  200.9 1.5 copy-start.6
  202.4 120.1 %all-gather.11.cloned.1.call-start = ((), (), s32[]{:S(2)}) async-start(), calls=%async_computation.1 | async-start | bytes 5242880 | tf_op jit(solution)/shard_map/all_gather | solution.py:180
  203.8 118.7 %copy-start.1 = (bf16[384,2048]{1,0:T(8,128)(2,1)S(1)}, bf16[384,2048]{1,0:T(8,128)(2,1)}, u32[]{:S(2)}) copy-start(bf16[384,2048]{1,0:T(8,128)(2,1)} %copy-done) | copy-start | bytes 4718596
Sparse Core Ops, SparseCore 0:
  8.9 22.3 all-gather.8
  32.9 36.9 all-gather.14
  71.5 36.1 all-gather.16
  109.1 34.4 all-gather.18
  145.1 27.0 all-gather.12
  173.6 45.0 all-gather.22
  220.2 19.9 all-gather.20
  241.7 80.7 all-gather.10
where the time goes:
time: 341 us; the launch traced here: 340 us
  waiting for transfers between devices  134 us (39%)
  blocking collectives  107 us (31%)
  matrix products  37.9 us (11%)
  other arithmetic  23.1 us (7%)
  local copies, waits for them, and re-layouts  16.3 us (5%)
  between operations  14.7 us (4%)
  starting transfers between devices  6.38 us (2%)
    all_gather x1, waiting for transfers between devices, on_device(): lax.all_gather(merge_flat, 'sp', axis=0, tiled=True)  79.3 us
    all_gather x1, blocking collectives, forget_groups(): key_rows = lax.all_gather(keys, 'sp', axis=0, tiled=True)  25.4 us
    all_gather x1, blocking collectives, forget_groups(): value_rows = lax.all_gather(values, 'sp', axis=0, tiled=True)  25.2 us
    all_gather x1, waiting for transfers between devices, on_device(): lax.all_gather(head_stack, 'tp', axis=2, tiled=True)  21.5 us
    all_gather x1, blocking collectives, on_device(): lax.all_gather(w_value_window, 'sp', axis=0, tiled=True)  21.1 us
    all_gather x1, blocking collectives, on_device(): lax.all_gather(w_key_window, 'sp', axis=0, tiled=True)  19 us
    dot_general x7, matrix products, on_device(): jnp.dot(normed, weight_rows, preferred_element_type=jnp.float32)  16.8 us
    all_gather x1, blocking collectives, forget_groups(): gates_all = lax.all_gather(gates, 'sp', axis=0, tiled=True)  16.6 us
  transfers between devices with their start and end apart: 10, of which 6 were waited for; matrix products, arithmetic and copies ran while one was open for 20% of the time, Pallas kernels for 0%

commit v1 on v0

--- a/solution.py
+++ b/solution.py
@@ -209,9 +209,10 @@
     branch_full = lax.all_gather(w_branch, "sp", axis=1, tiled=True)
     head_stack = jnp.stack([window_out, forget_out], axis=1)
     weight_rows = branch_full
+    register_wires_in = lambda own_rows: jnp.concatenate(lax.all_gather(own_rows, "tp"), axis=2)
     projection = jnp.einsum(
         "uxa,xag->uxg",
-        lax.all_gather(head_stack, "tp", axis=2, tiled=True),
+        register_wires_in(head_stack),
         weight_rows,
         preferred_element_type=jnp.float32,
     )

time: 341 us -> 381 us (1.12)
  waiting for transfers between devices: 134 us -> 177 us
  local copies, waits for them, and re-layouts: 16.3 us -> 21.4 us
  other arithmetic: 23.1 us -> 18.3 us
    all_gather x1, waiting for transfers between devices: 14.9 us -> 44.4 us  [on_device(): branch_full = lax.all_gather(w_branch, 'sp', axis=1, tiled=True)]
    all_gather x1, waiting for transfers between devices: 8.71 us -> 24.1 us  [on_device(): lax.all_gather(w_query_forget, 'sp', axis=0, tiled=True)]
    all_gather x1, waiting for transfers between devices: 21.5 us -> 17.4 us  [on_device(): lax.all_gather(own_rows, 'tp')]
  transfers between devices with their start and end apart: 10 -> 10, of which waited for: 6 -> 5; matrix products, arithmetic and copies ran while one was open for 20% -> 14% of each run, Pallas kernels for 0% -> 0%
where the time goes in v1:
time: 381 us; the launch traced here: 380 us
  waiting for transfers between devices  177 us (46%)
  blocking collectives  105 us (28%)
  matrix products  36.7 us (10%)
  local copies, waits for them, and re-layouts  21.4 us (6%)
  other arithmetic  18.3 us (5%)
  between operations  14.6 us (4%)
  starting transfers between devices  7.2 us (2%)
    all_gather x1, waiting for transfers between devices, on_device(): lax.all_gather(merge_flat, 'sp', axis=0, tiled=True)  78.1 us
    all_gather x1, waiting for transfers between devices, on_device(): branch_full = lax.all_gather(w_branch, 'sp', axis=1, tiled=True)  44.4 us
    all_gather x1, blocking collectives, forget_groups(): value_rows = lax.all_gather(values, 'sp', axis=0, tiled=True)  25.3 us
    all_gather x1, blocking collectives, forget_groups(): key_rows = lax.all_gather(keys, 'sp', axis=0, tiled=True)  25 us
    all_gather x1, waiting for transfers between devices, on_device(): lax.all_gather(w_query_forget, 'sp', axis=0, tiled=True)  24.1 us
    all_gather x1, blocking collectives, on_device(): lax.all_gather(w_value_window, 'sp', axis=0, tiled=True)  22.7 us
    all_gather x1, waiting for transfers between devices, on_device(): lax.all_gather(own_rows, 'tp')  17.4 us
    all_gather x1, blocking collectives, on_device(): lax.all_gather(w_key_window, 'sp', axis=0, tiled=True)  17.2 us
  transfers between devices with their start and end apart: 10, of which 5 were waited for; matrix products, arithmetic and copies ran while one was open for 14% of the time, Pallas kernels for 0%

profile of v1, /device:TPU:0, one launch (start us, length us, event | category | flops | bytes accessed | tf_op | source)
XLA Modules:
  0.0 380.1 jit_solution(18097175595683494817)
XLA Ops:
  6.5 0.7 all-gather.10.cloned.1.call-update
  7.3 0.7 all-gather.16.cloned.1.call-update
  8.1 0.7 all-gather.20.cloned.1.call-update
  11.2 0.8 slice_bitcast_fusion.2
  12.1 15.1 %all_gather.51 = f32[1536,4]{0,1:T(4,128)S(1)} all-gather(f32[384,4]{0,1:T(4,128)} %param.27), channel_id=1, replica_groups=mesh['grp'=2,'sp'=4,'tp'=4] {'sp'}, dimensions={0}, use_global_device_ids=true | all-gather | bytes 30720 | tf_op jit(solution)/shard_map/all_gather | solution.py:76
  27.3 17.2 %all_gather.45 = bf16[2048,128]{1,0:T(8,128)(2,1)} all-gather(bf16[512,128]{1,0:T(8,128)(2,1)S(1)} %copy-done.10), channel_id=1, replica_groups=mesh['grp'=2,'sp'=4,'tp'=4] {'sp'}, dimensions={0}, use_global_device_ids=true | all-gather | bytes 655360 | tf_op jit(solution)/shard_map/all_gather | solution.py:175
  44.6 22.7 %all_gather.44 = bf16[2048,128]{1,0:T(8,128)(2,1)S(1)} all-gather(bf16[512,128]{1,0:T(8,128)(2,1)S(1)} %copy-done.11), channel_id=1, replica_groups=mesh['grp'=2,'sp'=4,'tp'=4] {'sp'}, dimensions={0}, use_global_device_ids=true | all-gather | bytes 655360 | tf_op jit(solution)/shard_map/all_gather | solution.py:176
  67.3 0.7 broadcast_and_fusion
  68.0 1.9 fusion.25
  70.9 0.9 reshape.282
  71.8 0.6 slice.65
  72.4 2.0 multiply_reduce_fusion.1
  74.5 24.1 %all-gather.20.cloned.1.call-done = bf16[2048,256]{1,0:T(8,128)(2,1)} async-done(((bf16[512,256]{1,0:T(8,128)(2,1)}), bf16[2048,256]{1,0:T(8,128)(2,1)}) %all-gather.20.cloned.1.call-update) | async-done | bytes 1048592 | tf_op jit(solution)/shard_map/all_gather | solution.py:177
  98.7 2.0 multiply_reduce_fusion
  100.7 0.8 multiply_convert_fusion.1
  101.5 25.0 %all_gather.48 = bf16[1536,4,64]{0,2,1:T(8,128)(2,1)S(1)} all-gather(bf16[384,4,64]{0,2,1:T(8,128)(2,1)S(1)} %multiply_convert_fusion.2), channel_id=1, replica_groups=mesh['grp'=2,'sp'=4,'tp'=4] {'sp'}, dimensions={0}, use_global_device_ids=true | all-gather | bytes 983040 | tf_op jit(solution)/shard_map/all_gather | solution.py:115
  126.4 8.7 %all-gather.18.cloned.1.call-done = bf16[2048,256]{1,0:T(8,128)(2,1)} async-done(((bf16[512,256]{1,0:T(8,128)(2,1)}), bf16[2048,256]{1,0:T(8,128)(2,1)}) %all-gather.18.cloned.1.call-update) | async-done | bytes 1048592 | tf_op jit(solution)/shard_map/all_gather | solution.py:179
  135.1 2.0 convolution_convert_fusion.1
  137.1 25.3 %all_gather.50 = bf16[1536,4,64]{0,2,1:T(8,128)(2,1)S(1)} all-gather(bf16[384,4,64]{0,2,1:T(8,128)(2,1)S(1)} %bitcast.172), channel_id=1, replica_groups=mesh['grp'=2,'sp'=4,'tp'=4] {'sp'}, dimensions={0}, use_global_device_ids=true | all-gather | bytes 983040 | tf_op jit(solution)/shard_map/all_gather | solution.py:116
  162.4 22.7 %conditional.1 = (f32[4,384]{1,0:T(4,128)}, f32[384,4,64]{0,2,1:T(8,128)}) conditional(s32[]{:T(128)} %bitcast.13, () %tuple.20, (bf16[1536,4,64]{0,2,1:T(8,128)(2,1)S(1)}, bf16[1536,4,64]{0,2,1:T(8,128)(2,1)S(1)}, f32[1536,4]{0,1:T(4,128)S(1)}, s32[3,512]{1,0:T(4,128)S(1)}, s32[3,512]{1,0:T(4,128)S(1)}, /*index=5*/s32[384]{0:T(512)S(1)}, ...), branch_computations={%region_7.8_spmd, %region_8.13_spmd} | conditional | flops 215199744 | bytes 15060769 | solution.py:138
  162.5 1.3 copy_bitcast_fusion
  163.8 21.3 %while.18 = (s32[]{:T(128)}, f32[4,384]{1,0:T(4,128)S(1)}, f32[4,384]{1,0:T(4,128)}, f32[384,4,64]{0,2,1:T(8,128)}, s32[384]{0:T(512)S(1)}, /*index=5*/s32[3,512...) while((s32[]{:T(128)}, f32[4,384]{1,0:T(4,128)S(1)}, ...), condition=%wide.region_12.12_spmd.clone, body=%wide.region_9.11_spmd.clone.sunk | while | flops 215196672 | bytes 11896481 | solution.py:133
  164.0 2.0 fusion.85
  166.1 0.9 fusion.87
  167.0 0.6 fusion.88
  167.6 2.7 fusion.89
  170.6 2.0 fusion.85
  172.6 0.9 fusion.87
  173.6 1.3 fusion.88
  174.9 2.9 fusion.89
  177.9 2.0 fusion.85
  180.0 0.9 fusion.87
  180.9 1.3 fusion.88
  182.2 2.9 fusion.89
  185.1 1.0 divide_convert_fusion.2
  186.1 0.8 copy.61
  186.9 2.5 bitcast_reduce_fusion
  190.9 0.6 multiply_reduce_fusion.2
  191.9 2.4 collective-permute-start.1
  194.3 1.7 copy.51
  195.9 4.5 %collective-permute-start = (bf16[128,2,64]{0,2,1:T(8,128)(2,1)}, bf16[128,2,64]{0,2,1:T(8,128)(2,1)S(1)}, u32[]{:S(2)}, u32[]{:S(2)}) collective-permute-start(bf16[128,2,64]{0,2,1:T(8,128)(2,1)} %bitcast.1), channel_id=1, source_target_pairs={{0,4},{4,8},{8,12},{1,5},{5,9},{9,13},{2,6},{6,10},{10,14},{3,7},{... | collective-permute-start | bytes 98312 | tf_op jit(solution)/shard_map/ppermute | solution.py:16
  200.5 1.7 multiply_convert_fusion
  202.1 0.8 fusion.46
  203.5 1.6 fusion.28
  205.2 0.6 fusion.31
  205.8 0.7 exponential_add_fusion
  206.5 0.7 fusion.49
  207.2 1.1 reshape.267
  208.3 0.7 copy.50
  209.0 1.1 reshape.266
  210.2 2.5 fusion.32
  212.7 1.3 copy.60
  214.3 0.8 pad_maximum_fusion
  215.2 0.7 all-gather.22.cloned.1.call-update
  216.0 1.2 copy.76
  217.2 17.4 %all-gather.24.cloned.1.call-done = bf16[1536,2,256]{2,0,1:T(8,128)(2,1)} async-done(((bf16[384,2,256]{2,0,1:T(8,128)(2,1)}), bf16[1536,2,256]{2,0,1:T(8,128)(2,1)}) %all-gather.24.cloned.1.call-update) | async-done | bytes 1572880 | tf_op jit(solution)/shard_map/all_gather | solution.py:212
  234.6 2.9 copy.75
  237.5 44.4 %all-gather.22.cloned.1.call-done = bf16[2,1024,512]{2,1,0:T(8,128)(2,1)} async-done(((bf16[2,256,512]{2,1,0:T(8,128)(2,1)}), bf16[2,1024,512]{2,1,0:T(8,128)(2,1)}) %all-gather.22.cloned.1.call-update) | async-done | bytes 2097168 | tf_op jit(solution)/shard_map/all_gather | solution.py:209
  281.9 3.0 convolution_bitcast_fusion
  284.9 78.1 %all-gather.12.cloned.1.call-done = bf16[2048,1024]{1,0:T(8,128)(2,1)} async-done(((bf16[512,1024]{1,0:T(8,128)(2,1)}), bf16[2048,1024]{1,0:T(8,128)(2,1)}) %all-gather.12.cloned.1.call-update) | async-done | bytes 4194320 | tf_op jit(solution)/shard_map/all_gather | solution.py:180
  363.0 5.3 %add_divide_fusion = f32[384,1024]{1,0:T(8,128)} fusion(bf16[384,2048]{1,0:T(8,128)(2,1)S(1)} %copy-done.1, bf16[2048,1024]{1,0:T(8,128)(2,1)} %all-gather.12.cloned.1.call-done), kind=kOutput, calls=%fused_computation.44 | convolution fusion | flops 1611792384 | bytes 7340032 | tf_op jit(solution)/shard_map/dot_general | solution.py:183
  368.3 2.6 reshape.264
  371.0 1.2 fusion.56
  372.2 1.0 fusion.36
  (100 shorter events, 6.6 us)
Async XLA Ops:
  6.5 20.8 %copy-start.10 = (bf16[512,128]{1,0:T(8,128)(2,1)S(1)}, bf16[512,128]{1,0:T(8,128)(2,1)}, u32[]{:S(2)}) copy-start(bf16[512,128]{1,0:T(8,128)(2,1)} %param.21) | copy-start | bytes 393220
  6.5 37.9 %copy-start.14 = (f32[4]{0:T(128)S(1)}, f32[4]{0:T(128)}, u32[]{:S(2)}) copy-start(f32[4]{0:T(128)} %param.23) | copy-start | bytes 52
  6.5 38.0 %copy-start.11 = (bf16[512,128]{1,0:T(8,128)(2,1)S(1)}, bf16[512,128]{1,0:T(8,128)(2,1)}, u32[]{:S(2)}) copy-start(bf16[512,128]{1,0:T(8,128)(2,1)} %param.22) | copy-start | bytes 393220
  6.5 61.4 %all-gather.10.cloned.1.call-start = ((), (), s32[]{:S(2)}) async-start(), calls=%async_computation | async-start | bytes 1966080 | tf_op jit(solution)/shard_map/all_gather | solution.py:165
  7.3 65.2 %all-gather.16.cloned.1.call-start = ((), (), s32[]{:S(2)}) async-start(), calls=%async_computation.3 | async-start | bytes 1310720 | tf_op jit(solution)/shard_map/all_gather | solution.py:178
  8.0 90.6 %all-gather.20.cloned.1.call-start = ((), (), s32[]{:S(2)}) async-start(), calls=%async_computation.5 | async-start | bytes 1310720 | tf_op jit(solution)/shard_map/all_gather | solution.py:177
  8.7 126.4 %all-gather.18.cloned.1.call-start = ((), (), s32[]{:S(2)}) async-start(), calls=%async_computation.4 | async-start | bytes 1310720 | tf_op jit(solution)/shard_map/all_gather | solution.py:179
  9.3 177.6 %all-gather.14.cloned.1.call-start = ((), (), s32[]{:S(2)}) async-start(), calls=%async_computation.2 | async-start | bytes 1310720 | tf_op jit(solution)/shard_map/all_gather | solution.py:174
  9.9 60.0 %copy-start.13 = (f32[2048]{0:T(1024)S(1)}, f32[2048]{0:T(1024)}, u32[]{:S(2)}) copy-start(f32[2048]{0:T(1024)} %param.18) | copy-start | bytes 24580
  9.9 224.7 %all-gather.24.cloned.1.call-start = ((), (), s32[]{:S(2)}) async-start(), calls=%async_computation.7 | async-start | bytes 1966080 | tf_op jit(solution)/shard_map/all_gather | solution.py:212
  67.9 1.9 copy-start.2
  70.3 64.8 %copy-start = (bf16[384,2048]{1,0:T(8,128)(2,1)}, bf16[384,2048]{1,0:T(8,128)(2,1)S(1)}, u32[]{:S(2)}) copy-start(bf16[384,2048]{1,0:T(8,128)(2,1)S(1)} %fusion.27) | copy-start | bytes 4718596
  70.9 29.7 %copy-start.4 = (bf16[384,128]{0,1:T(8,128)(2,1)}, bf16[384,128]{0,1:T(8,128)(2,1)S(1)}, u32[]{:S(2)}) copy-start(bf16[384,128]{0,1:T(8,128)(2,1)S(1)} %convolution_convert_fusion.2) | copy-start | bytes 294916
  126.4 36.0 %copy-start.9 = (f32[384,4]{0,1:T(4,128)S(1)}, f32[384,4]{0,1:T(4,128)}, u32[]{:S(2)}) copy-start(f32[384,4]{0,1:T(4,128)} %param.27) | copy-start | bytes 18436
  189.4 1.4 copy-start.1
  189.4 1.5 copy-start.3
  191.9 11.0 %collective-permute-start.1 = (bf16[128,2,64]{0,2,1:T(8,128)(2,1)S(1)}, bf16[128,2,64]{0,2,1:T(8,128)(2,1)S(1)}, u32[]{:S(2)}, u32[]{:S(2)}) collective-permute-start(bf16[128,2,64]{0,2,1:T(8,128)(2,1)S(1)} %slice.68), channel_id=1, source_target_pairs={{0,4},{4,8},{8,12},{1,5},{5,9},{9,13},{2,6},{6,10},{10,14},{3,7},{... | collective-permute-start | bytes 98312 | tf_op jit(solution)/shard_map/ppermute | solution.py:16
  195.9 10.6 %collective-permute-start = (bf16[128,2,64]{0,2,1:T(8,128)(2,1)}, bf16[128,2,64]{0,2,1:T(8,128)(2,1)S(1)}, u32[]{:S(2)}, u32[]{:S(2)}) collective-permute-start(bf16[128,2,64]{0,2,1:T(8,128)(2,1)} %bitcast.1), channel_id=1, source_target_pairs={{0,4},{4,8},{8,12},{1,5},{5,9},{9,13},{2,6},{6,10},{10,14},{3,7},{... | collective-permute-start | bytes 98312 | tf_op jit(solution)/shard_map/ppermute | solution.py:16
  202.1 1.3 copy-start.8
  205.1 1.4 copy-start.5
  207.2 2.9 copy-start.12
  210.2 4.2 %copy-start.7 = (bf16[384,1,256]{2,0,1:T(8,128)(2,1)S(1)}, bf16[384,1,256]{2,0,1:T(8,128)(2,1)}, u32[]{:S(2)}) copy-start(bf16[384,1,256]{2,0,1:T(8,128)(2,1)} %copy.61) | copy-start | bytes 589828
  212.7 3.2 copy-start.6
  215.2 66.7 %all-gather.22.cloned.1.call-start = ((), (), s32[]{:S(2)}) async-start(), calls=%async_computation.6 | async-start | bytes 2621440 | tf_op jit(solution)/shard_map/all_gather | solution.py:209
  215.9 147.1 %all-gather.12.cloned.1.call-start = ((), (), s32[]{:S(2)}) async-start(), calls=%async_computation.1 | async-start | bytes 5242880 | tf_op jit(solution)/shard_map/all_gather | solution.py:180
Sparse Core Ops, SparseCore 0:
  8.9 22.3 all-gather.9
  32.8 36.4 all-gather.15
  70.9 27.7 all-gather.19
  100.1 35.0 all-gather.17
  136.6 34.3 all-gather.13
  215.3 19.2 all-gather.23
  236.2 45.6 all-gather.21
  283.4 79.5 all-gather.11
